TPU v7x, 32 devices: a whole 2x2x4 slice. The times are simulated.
32 devices in a mesh: fs: 4 (over z), rep: 4 (over y, x), tp: 2 (over core).
Axes of the slice: x: 2, y: 2, z: 4, core: 2. Of those that a mesh axis runs over, the one named last changes fastest.
Arguments:
- saved_input: bfloat16 [16384, 2048], P(('fs', 'rep')), may hold values from -500 to 500
- query_cotangent: bfloat16 [16384, 2048], P(('fs', 'rep'), 'tp'), may hold values from -0.014038086 to 0.014038086
- key_cotangent: bfloat16 [16384, 512], P(('fs', 'rep'), 'tp'), may hold values from -0.014038086 to 0.014038086
- query_weight: float32 [2048, 2048], P('fs', 'tp'), may hold values from -45 to 45
- key_weight: float32 [2048, 512], P('fs', 'tp'), may hold values from -45 to 45
- query_moment: float32 [2048, 2048], P('fs', 'tp'), may hold values from -45 to 45
- key_moment: float32 [2048, 512], P('fs', 'tp'), may hold values from -45 to 45
- query_row_root: bfloat16 [2048, 2048], P('fs'), may hold values from -1 to 3, as said below
- key_row_root: bfloat16 [2048, 2048], P('fs'), may hold values from -1 to 3, as said below
- query_head_root: bfloat16 [32, 64, 64], P('tp'), may hold values from -1 to 3, as said below
- key_head_root: bfloat16 [8, 64, 64], P('tp'), may hold values from -1 to 3, as said below
- query_head_stat: float32 [32, 64, 64], P('tp'), may hold values from -26 to 27, as said below
- key_head_stat: float32 [8, 64, 64], P('tp'), may hold values from -26 to 27, as said below
Outputs:
- query_step: float32 [2048, 2048], P('fs', 'tp')
- key_step: float32 [2048, 512], P('fs', 'tp')
- query_next: float32 [2048, 2048], P('fs', 'tp')
- key_next: float32 [2048, 512], P('fs', 'tp')
- query_copy: bfloat16 [2048, 2048], P(None, 'tp')
- key_copy: bfloat16 [2048, 512], P(None, 'tp')
- query_moment_next: float32 [2048, 2048], P('fs', 'tp')
- key_moment_next: float32 [2048, 512], P('fs', 'tp')
- query_stat_next: float32 [32, 64, 64], P('tp')
- key_stat_next: float32 [8, 64, 64], P('tp')
Inputs may be any that keep to these rules, and one draw needn't show every extreme that they name: `query_row_root`: symmetric. `key_row_root`: symmetric. `query_head_root`: each head's matrix is symmetric. `key_head_root`: each head's matrix is symmetric. `query_head_stat`: each head's matrix is symmetric. `key_head_stat`: each head's matrix is symmetric.
All inputs are finite; a program needn't handle non-finite values.
Results may differ from a plain program's by a relative error of at most 0.0018.
The roundings to bfloat16 on the way count: a program that leaves them out, or rounds other values in their place, can miss the bound.
Values may be sent and summed in bfloat16 or wider, within the bound.
A program may use at most 128 MiB of HBM per device.

v0:
```python
import jax
import jax.numpy as jnp
from jax import lax
from jax.sharding import PartitionSpec as P

D = 2048
HEAD_DIM = 64
MOMENT_DECAY = 0.8
STAT_DECAY = 0.5
LEARN_RATE = 0.1
EPSILON = 1e-06


def head_gram(rounded, head_count):
    shaped = rounded.reshape(rounded.shape[0], head_count, HEAD_DIM)
    return jnp.einsum("rhd,rhe->hde", shaped, shaped, preferred_element_type=jnp.float32)


def column_factor(rounded, head_root):
    head_count = head_root.shape[0]
    shaped = rounded.reshape(rounded.shape[0], head_count, HEAD_DIM)
    rightward = jnp.einsum("rhd,hde->rhe", shaped, head_root, preferred_element_type=jnp.float32)
    return rightward.reshape(rounded.shape[0], head_count * HEAD_DIM).astype(jnp.bfloat16)


def shards(
    saved_input,
    query_cotangent,
    key_cotangent,
    query_weight,
    key_weight,
    query_moment,
    key_moment,
    query_row_root,
    key_row_root,
    query_head_root,
    key_head_root,
    query_head_stat,
    key_head_stat,
):
    query_width = query_cotangent.shape[1]
    cotangents = jnp.concatenate([query_cotangent, key_cotangent], axis=1)
    partial_value = lax.psum_scatter(
        lax.dot_general(
            saved_input, cotangents, (((0,), (0,)), ((), ())), preferred_element_type=jnp.float32
        ),
        ("fs", "rep"),
        scatter_dimension=0,
        tiled=True,
    )
    gradient = lax.all_gather(partial_value, "rep", axis=0, tiled=True)
    rounded = gradient.astype(jnp.bfloat16)
    query_rounded = rounded[:, :query_width]
    key_rounded = rounded[:, query_width:]
    query_gram, key_gram = lax.psum(
        (
            head_gram(query_rounded, query_head_root.shape[0]),
            head_gram(key_rounded, key_head_root.shape[0]),
        ),
        "fs",
    )
    query_stat_next = STAT_DECAY * query_head_stat + (1.0 - STAT_DECAY) * query_gram / D
    key_stat_next = STAT_DECAY * key_head_stat + (1.0 - STAT_DECAY) * key_gram / D
    query_right = column_factor(query_rounded, query_head_root)
    key_right = column_factor(key_rounded, key_head_root)
    query_piece = lax.all_gather(query_right, "fs", axis=0, tiled=True)
    key_piece = lax.all_gather(key_right, "fs", axis=0, tiled=True)
    query_pre = jnp.dot(query_row_root, query_piece, preferred_element_type=jnp.float32)
    key_pre = jnp.dot(key_row_root, key_piece, preferred_element_type=jnp.float32)
    query_moment_next = MOMENT_DECAY * query_moment + (1.0 - MOMENT_DECAY) * query_pre
    key_moment_next = MOMENT_DECAY * key_moment + (1.0 - MOMENT_DECAY) * key_pre
    query_wsq, query_msq, key_wsq, key_msq = lax.psum(
        (
            jnp.sum(query_weight * query_weight),
            jnp.sum(query_moment_next * query_moment_next),
            jnp.sum(key_weight * key_weight),
            jnp.sum(key_moment_next * key_moment_next),
        ),
        ("fs", "tp"),
    )
    query_step = (
        LEARN_RATE * (jnp.sqrt(query_wsq) / jnp.sqrt(query_msq + EPSILON)) * query_moment_next
    )
    key_step = LEARN_RATE * (jnp.sqrt(key_wsq) / jnp.sqrt(key_msq + EPSILON)) * key_moment_next
    query_next = query_weight - query_step
    key_next = key_weight - key_step
    query_copy, key_copy = (
        lax.all_gather(query_next.astype(jnp.bfloat16), "fs", axis=0, tiled=True),
        lax.all_gather(key_next.astype(jnp.bfloat16), "fs", axis=0, tiled=True),
    )
    return (
        query_step,
        key_step,
        query_next,
        key_next,
        query_copy,
        key_copy,
        query_moment_next,
        key_moment_next,
        query_stat_next,
        key_stat_next,
    )


def solution(mesh):
    in_specs = (
        P(("fs", "rep"), None),
        P(("fs", "rep"), "tp"),
        P(("fs", "rep"), "tp"),
        P("fs", "tp"),
        P("fs", "tp"),
        P("fs", "tp"),
        P("fs", "tp"),
        P("fs", None),
        P("fs", None),
        P("tp", None, None),
        P("tp", None, None),
        P("tp", None, None),
        P("tp", None, None),
    )
    out_specs = (
        P("fs", "tp"),
        P("fs", "tp"),
        P("fs", "tp"),
        P("fs", "tp"),
        P(None, "tp"),
        P(None, "tp"),
        P("fs", "tp"),
        P("fs", "tp"),
        P("tp", None, None),
        P("tp", None, None),
    )
    return jax.shard_map(shards, mesh=mesh, in_specs=in_specs, out_specs=out_specs, check_vma=False)
```

profile of v0, /device:TPU:0, one launch (start us, length us, event | category | flops | bytes accessed | tf_op | source)
XLA Modules:
  0.0 567.2 jit_solution(7115571609931742830)
XLA Ops:
  7.2 0.0 copy-start
  7.2 0.0 reduce-scatter.2.cloned.1.call-start
  7.2 10.8 %convolution_bitcast_fusion = f32[2048,1280]{0,1:T(8,128)} fusion(bf16[1024,2048]{1,0:T(8,128)(2,1)} %param.13, bf16[1024,256]{1,0:T(8,128)(2,1)} %param.15, bf16[1024,1024]{1,0:T(8,128)(2,1)} %param.14), kind=kOutput, calls=%fused_computation | convolution fusion | flops 5373952000 | bytes 17301504 | tf_op jit(solution)/shard_map/dot_general | solution.py:44
  18.0 0.0 reduce-scatter.2.cloned.1.call-update
  18.0 0.0 all-gather.6.cloned.1.call-start
  18.1 222.6 %reduce-scatter.2.cloned.1.call-done = f32[128,1280]{0,1:T(8,128)} async-done(((f32[2048,1280]{0,1:T(8,128)}), f32[128,1280]{0,1:T(8,128)}) %reduce-scatter.2.cloned.1.call-update) | async-done | bytes 655376 | tf_op jit(solution)/shard_map/reduce_scatter | solution.py:43
  240.7 0.0 all-gather.6.cloned.1.call-update
  240.7 0.0 copy-start.7
  240.7 0.0 all-gather.10.cloned.1.call-start
  240.8 44.8 %all-gather.6.cloned.1.call-done = f32[512,1280]{0,1:T(8,128)} async-done(((f32[128,1280]{0,1:T(8,128)}), f32[512,1280]{0,1:T(8,128)}) %all-gather.6.cloned.1.call-update) | async-done | bytes 2621456 | tf_op jit(solution)/shard_map/all_gather | solution.py:51
  285.6 1.9 convert_element_type.27
  287.5 0.0 copy-start.4
  287.5 1.0 copy-done.4
  288.6 0.0 copy-done.7
  288.6 1.0 convolution_convert_fusion.1
  289.5 0.0 all-gather.10.cloned.1.call-update
  289.6 0.0 all-gather.8.cloned.1.call-start
  289.6 1.3 slice.8
  290.9 2.4 convolution_convert_fusion
  293.3 0.0 all-gather.8.cloned.1.call-update
  293.3 0.0 all-reduce.4.cloned.1.call-start
  293.4 2.9 copy.23
  296.3 2.1 copy.25
  298.3 2.0 copy.28
  300.4 1.8 multiply_reduce_fusion.3
  302.2 2.7 multiply_reduce_fusion.1
  304.9 0.9 fusion.9
  305.8 1.2 fusion.8
  307.0 0.0 all-reduce.4.cloned.1.call-update
  307.0 0.0 all-gather.14.cloned.1.call-start
  307.0 10.7 %all-gather.10.cloned.1.call-done = bf16[2048,256]{0,1:T(8,128)(2,1)} async-done(((bf16[512,256]{0,1:T(8,128)(2,1)}), bf16[2048,256]{0,1:T(8,128)(2,1)}) %all-gather.10.cloned.1.call-update) | async-done | bytes 1048592 | tf_op jit(solution)/shard_map/all_gather | solution.py:67
  317.7 3.4 multiply_reduce_fusion.2
  321.1 78.7 %all-gather.8.cloned.1.call-done = bf16[2048,1024]{0,1:T(8,128)(2,1)} async-done(((bf16[512,1024]{0,1:T(8,128)(2,1)}), bf16[2048,1024]{0,1:T(8,128)(2,1)}) %all-gather.8.cloned.1.call-update) | async-done | bytes 4194320 | tf_op jit(solution)/shard_map/all_gather | solution.py:66
  399.8 0.0 copy-done
  399.8 7.2 %multiply_reduce_fusion = (f32[]{:T(128)}, f32[512,1024]{0,1:T(8,128)}) fusion(bf16[2048,1024]{0,1:T(8,128)(2,1)} %all-gather.8.cloned.1.call-done, bf16[512,2048]{1,0:T(8,128)(2,1)S(1)} %copy-done, f32[512,1024]{0,1:T(8,128)} %copy.23), kind=kOutput, calls=%fused_computation.5 | convolution fusion | flops 2150105088 | bytes 10485764 | tf_op jit(solution)/shard_map/dot_general | solution.py:68
  407.1 14.9 %all-reduce = (f32[]{:T(128)}, f32[]{:T(128)}, f32[]{:T(128)}, f32[]{:T(128)}) all-reduce(f32[]{:T(128)} %multiply_reduce_fusion.1, f32[]{:T(128)} %get-tuple-element.32, f32[]{:T(128)} %multiply_reduce_fusion.3, f32[]{:T(128)} %get-tuple-element.34), channel_id=1, replica_groups=mesh['fs'=4,'rep'=4,'tp'=2] {'fs','tp'}, use_global_device_ids=true, to_apply=%region_1.0 | all-reduce | flops 4 | bytes 32 | tf_op jit(solution)/shard_map/psum | solution.py:72
  423.4 2.1 fusion.6
  425.4 0.0 all-gather.14.cloned.1.call-update
  425.4 0.0 copy-start.2
  425.5 0.0 all-gather.12.cloned.1.call-start
  425.5 3.0 copy.27
  429.9 0.0 copy-done.2
  429.9 0.0 copy-start.6
  429.9 4.7 fusion.7
  434.6 0.0 all-gather.12.cloned.1.call-update
  434.6 8.0 %all-reduce.4.cloned.1.call-done = (f32[16,64,64]{2,1,0:T(8,128)}, f32[4,64,64]{2,1,0:T(8,128)}) async-done(((f32[16,64,64]{2,1,0:T(8,128)}, f32[4,64,64]{2,1,0:T(8,128)}), (f32[16,64,64]{2,1,0:T(8,128)}, f32[4,64,64]{2,1,0:T(8,128)})) %all-reduce.4.cloned.1.call-update) | async-done | bytes 327696 | tf_op jit(solution)/shard_map/psum | solution.py:55
  442.6 0.0 copy-done.6
  442.6 1.6 multiply_add_fusion.1
  444.2 2.1 multiply_add_fusion
  446.3 1.0 copy.36
  447.3 1.8 copy.35
  449.1 0.0 copy-start.5
  449.1 0.0 copy-start.3
  449.1 3.0 copy.29
  452.1 0.0 copy-done.5
  452.1 1.0 copy.30
  453.1 0.0 copy-done.3
  453.1 1.8 copy.31
  454.9 1.0 copy.32
  455.9 16.1 %all-gather.14.cloned.1.call-done = bf16[2048,256]{0,1:T(8,128)(2,1)} async-done(((bf16[512,256]{0,1:T(8,128)(2,1)}), bf16[2048,256]{0,1:T(8,128)(2,1)}) %all-gather.14.cloned.1.call-update) | async-done | bytes 1048592 | tf_op jit(solution)/shard_map/all_gather | solution.py:89
  472.1 2.3 copy.34
  474.3 79.5 %all-gather.12.cloned.1.call-done = bf16[2048,1024]{0,1:T(8,128)(2,1)} async-done(((bf16[512,1024]{0,1:T(8,128)(2,1)}), bf16[2048,1024]{0,1:T(8,128)(2,1)}) %all-gather.12.cloned.1.call-update) | async-done | bytes 4194320 | tf_op jit(solution)/shard_map/all_gather | solution.py:88
  553.8 6.5 %copy.33 = bf16[2048,1024]{1,0:T(8,128)(2,1)} copy(bf16[2048,1024]{0,1:T(8,128)(2,1)} %all-gather.12.cloned.1.call-done) | data formatting | bytes 8388608
  560.3 0.0 copy-done.1
  (2 shorter events, 0.0 us)
Async XLA Ops:
  7.2 392.7 %copy-start = (bf16[512,2048]{1,0:T(8,128)(2,1)S(1)}, bf16[512,2048]{1,0:T(8,128)(2,1)}, u32[]{:S(2)}) copy-start(bf16[512,2048]{1,0:T(8,128)(2,1)} %param.20) | copy-start | bytes 6291460
  7.2 233.5 %reduce-scatter.2.cloned.1.call-start = ((), (), s32[]{:S(2)}) async-start(), calls=%async_computation.1 | async-start | bytes 11141120 | tf_op jit(solution)/shard_map/reduce_scatter | solution.py:43
  18.0 267.5 %all-gather.6.cloned.1.call-start = ((), (), s32[]{:S(2)}) async-start(), calls=%async_computation.2 | async-start | bytes 3276800 | tf_op jit(solution)/shard_map/all_gather | solution.py:51
  240.7 47.8 %copy-start.7 = (bf16[4,64,64]{2,1,0:T(8,128)(2,1)S(1)}, bf16[4,64,64]{2,1,0:T(8,128)(2,1)}, u32[]{:S(2)}) copy-start(bf16[4,64,64]{2,1,0:T(8,128)(2,1)} %param.23) | copy-start | bytes 98308
  240.7 77.0 %all-gather.10.cloned.1.call-start = ((), (), s32[]{:S(2)}) async-start(), calls=%async_computation.4 | async-start | bytes 1310720 | tf_op jit(solution)/shard_map/all_gather | solution.py:67
  287.5 1.1 copy-start.4
  289.6 110.3 %all-gather.8.cloned.1.call-start = ((), (), s32[]{:S(2)}) async-start(), calls=%async_computation.3 | async-start | bytes 5242880 | tf_op jit(solution)/shard_map/all_gather | solution.py:66
  293.3 149.3 %all-reduce.4.cloned.1.call-start = ((), (), s32[]{:S(2)}) async-start(), calls=%async_computation.7 | async-start | bytes 1310720 | tf_op jit(solution)/shard_map/psum | solution.py:55
  307.0 165.1 %all-gather.14.cloned.1.call-start = ((), (), s32[]{:S(2)}) async-start(), calls=%async_computation.6 | async-start | bytes 1310720 | tf_op jit(solution)/shard_map/all_gather | solution.py:89
  425.4 4.5 copy-start.2
  425.5 128.3 %all-gather.12.cloned.1.call-start = ((), (), s32[]{:S(2)}) async-start(), calls=%async_computation.5 | async-start | bytes 5242880 | tf_op jit(solution)/shard_map/all_gather | solution.py:88
  429.9 12.7 %copy-start.6 = (f32[4,64,64]{2,1,0:T(8,128)S(1)}, f32[4,64,64]{2,1,0:T(8,128)}, u32[]{:S(2)}) copy-start(f32[4,64,64]{2,1,0:T(8,128)} %param.25) | copy-start | bytes 196612
  449.1 3.0 copy-start.5
  449.1 4.0 copy-start.3
  553.8 6.5 %copy-start.1 = (bf16[512,2048]{1,0:T(8,128)(2,1)S(1)}, bf16[512,2048]{1,0:T(8,128)(2,1)}, u32[]{:S(2)}) copy-start(bf16[512,2048]{1,0:T(8,128)(2,1)} %param.20) | copy-start | bytes 6291460
Sparse Core Ops, SparseCore 0:
  18.1 222.5 reduce-scatter.1
  242.5 42.9 all-gather.5
  289.7 27.9 all-gather.9
  319.7 80.1 all-gather.7
  403.3 39.3 all-reduce.3
  444.6 27.3 all-gather.13
  473.6 80.1 all-gather.11
where the time goes:
time: 568 us; the launch traced here: 567 us
  waiting for transfers between devices  460 us (81%)
  local copies, waits for them, and re-layouts  30.8 us (5%)
  matrix products  26.8 us (5%)
  between operations  17 us (3%)
  other arithmetic  16.8 us (3%)
  blocking collectives  14.9 us (3%)
    reduce_scatter x1, waiting for transfers between devices, shards(): lax.psum_scatter(lax.dot_general(saved_input, cotangents, (((0,), (0,)),...  223 us
    all_gather x1, waiting for transfers between devices, shards(): lax.all_gather(query_next.astype(jnp.bfloat16), 'fs', axis=0, tiled=True)  79.5 us
    all_gather x1, waiting for transfers between devices, shards(): query_piece = lax.all_gather(query_right, 'fs', axis=0, tiled=True)  78.7 us
    all_gather x1, waiting for transfers between devices, shards(): gradient = lax.all_gather(partial_value, 'rep', axis=0, tiled=True)  44.8 us
    unnamed x28, local copies, waits for them, and re-layouts  29.5 us
    all_gather x1, waiting for transfers between devices, shards(): lax.all_gather(key_next.astype(jnp.bfloat16), 'fs', axis=0, tiled=True)  16.1 us
    psum x1, blocking collectives, shards(): lax.psum((jnp.sum(query_weight * query_weight), jnp.sum(query_moment_next...  14.9 us
  transfers between devices with their start and end apart: 7, of which 7 were waited for; matrix products, arithmetic and copies ran while one was open for 9% of the time, Pallas kernels for 0%

commit v1 on v0

--- a/solution.py
+++ b/solution.py
@@ -63,7 +63,14 @@
     key_stat_next = STAT_DECAY * key_head_stat + (1.0 - STAT_DECAY) * key_gram / D
     query_right = column_factor(query_rounded, query_head_root)
     key_right = column_factor(key_rounded, key_head_root)
-    query_piece = lax.all_gather(query_right, "fs", axis=0, tiled=True)
+    size = lax.axis_size("fs")
+    route = [(i, (i + 1) % size) for i in range(size)]
+    parts = [query_right]
+    for stride in range(1, size):
+        parts = [lax.ppermute(parts[0], "fs", route), *parts]
+    out = jnp.concatenate(parts, axis=0)
+    shift = (lax.axis_index("fs") + 1) * parts[-1].shape[0]
+    query_piece = jnp.roll(out, shift, axis=0)
     key_piece = lax.all_gather(key_right, "fs", axis=0, tiled=True)
     query_pre = jnp.dot(query_row_root, query_piece, preferred_element_type=jnp.float32)
     key_pre = jnp.dot(key_row_root, key_piece, preferred_element_type=jnp.float32)

time: 568 us -> 543 us (0.956)
  waiting for transfers between devices: 460 us -> 430 us
  local copies, waits for them, and re-layouts: 30.8 us -> 40.3 us
    ppermute x0 -> x3, waiting for transfers between devices: none -> 82.9 us  [shards(): parts = [lax.ppermute(parts[0], 'fs', route), *parts]]
    all_gather x1 -> x0, waiting for transfers between devices: 78.7 us -> none  [shards(): query_piece = lax.all_gather(query_right, 'fs', axis=0, tiled=True)]
    all_gather x1, waiting for transfers between devices: 16.1 us -> 0.22 us  [shards(): lax.all_gather(key_next.astype(jnp.bfloat16), 'fs', axis=0, tiled=True)]
    all_gather x1, waiting for transfers between devices: 10.7 us -> 0.02 us  [shards(): key_piece = lax.all_gather(key_right, 'fs', axis=0, tiled=True)]
    unnamed x28 -> x41, local copies, waits for them, and re-layouts: 29.5 us -> 40.1 us
    psum x1, waiting for transfers between devices: 7.98 us -> 0.02 us  [shards(): lax.psum((head_gram(query_rounded, query_head_root.shape[0]), head_gram(k...]
  transfers between devices with their start and end apart: 7 -> 9, of which waited for: 7 -> 7; matrix products, arithmetic and copies ran while one was open for 9% -> 11% of each run, Pallas kernels for 0% -> 0%
where the time goes in v1:
time: 543 us; the launch traced here: 542 us
  waiting for transfers between devices  430 us (79%)
  local copies, waits for them, and re-layouts  40.3 us (7%)
  matrix products  22.1 us (4%)
  between operations  17.1 us (3%)
  other arithmetic  16.6 us (3%)
  blocking collectives  14.3 us (3%)
    reduce_scatter x1, waiting for transfers between devices, shards(): lax.psum_scatter(lax.dot_general(saved_input, cotangents, (((0,), (0,)),...  223 us
    ppermute x3, waiting for transfers between devices, shards(): parts = [lax.ppermute(parts[0], 'fs', route), *parts]  82.9 us
    all_gather x1, waiting for transfers between devices, shards(): lax.all_gather(query_next.astype(jnp.bfloat16), 'fs', axis=0, tiled=True)  79.3 us
    all_gather x1, waiting for transfers between devices, shards(): gradient = lax.all_gather(partial_value, 'rep', axis=0, tiled=True)  44.8 us
    unnamed x41, local copies, waits for them, and re-layouts  40.1 us
    psum x1, blocking collectives, shards(): lax.psum((jnp.sum(query_weight * query_weight), jnp.sum(query_moment_next...  14.3 us
  transfers between devices with their start and end apart: 9, of which 7 were waited for; matrix products, arithmetic and copies ran while one was open for 11% of the time, Pallas kernels for 0%

profile of v1, /device:TPU:0, one launch (start us, length us, event | category | flops | bytes accessed | tf_op | source)
XLA Modules:
  0.0 542.3 jit_solution(5506679058466528549)
XLA Ops:
  7.2 0.0 copy-start
  7.2 0.0 reduce-scatter.2.cloned.1.call-start
  7.2 10.8 %convolution_bitcast_fusion = f32[2048,1280]{0,1:T(8,128)} fusion(bf16[1024,2048]{1,0:T(8,128)(2,1)} %param.13, bf16[1024,256]{1,0:T(8,128)(2,1)} %param.15, bf16[1024,1024]{1,0:T(8,128)(2,1)} %param.14), kind=kOutput, calls=%fused_computation | convolution fusion | flops 5373952000 | bytes 17301504 | tf_op jit(solution)/shard_map/dot_general | solution.py:44
  18.0 0.0 reduce-scatter.2.cloned.1.call-update
  18.1 0.0 all-gather.5.cloned.1.call-start
  18.1 222.6 %reduce-scatter.2.cloned.1.call-done = f32[128,1280]{0,1:T(8,128)} async-done(((f32[2048,1280]{0,1:T(8,128)}), f32[128,1280]{0,1:T(8,128)}) %reduce-scatter.2.cloned.1.call-update) | async-done | bytes 655376 | tf_op jit(solution)/shard_map/reduce_scatter | solution.py:43
  240.7 0.0 all-gather.5.cloned.1.call-update
  240.8 0.0 all-gather.7.cloned.1.call-start
  240.8 44.8 %all-gather.5.cloned.1.call-done = f32[512,1280]{0,1:T(8,128)} async-done(((f32[128,1280]{0,1:T(8,128)}), f32[512,1280]{0,1:T(8,128)}) %all-gather.5.cloned.1.call-update) | async-done | bytes 2621456 | tf_op jit(solution)/shard_map/all_gather | solution.py:51
  285.6 1.9 convert_element_type.27
  287.5 0.0 copy-start.10
  287.5 0.1 slice.8
  287.6 0.5 convolution_convert_fusion
  288.1 1.0 copy-done.1
  289.1 1.5 collective-permute-start
  290.6 25.1 %collective-permute-done = bf16[512,1024]{0,1:T(8,128)(2,1)} collective-permute-done((bf16[512,1024]{0,1:T(8,128)(2,1)S(1)}, bf16[512,1024]{0,1:T(8,128)(2,1)}, u32[]{:S(2)}, u32[]{:S(2)}) %collective-permute-start) | collective-permute-done | bytes 1048608 | tf_op jit(solution)/shard_map/ppermute | solution.py:70
  315.7 1.0 convolution_convert_fusion.1
  316.7 0.0 all-gather.7.cloned.1.call-update
  316.7 0.0 all-reduce.4.cloned.1.call-start
  316.8 2.9 copy.23
  319.7 2.0 copy.25
  321.7 2.0 copy.28
  323.7 1.8 multiply_reduce_fusion.3
  325.5 30.5 %collective-permute-done.1 = bf16[512,1024]{0,1:T(8,128)(2,1)} collective-permute-done((bf16[512,1024]{0,1:T(8,128)(2,1)}, bf16[512,1024]{0,1:T(8,128)(2,1)}, u32[]{:S(2)}, u32[]{:S(2)}) %collective-permute-start.1) | collective-permute-done | bytes 1048608 | tf_op jit(solution)/shard_map/ppermute | solution.py:70
  356.1 2.7 multiply_reduce_fusion.1
  358.8 0.9 fusion.14
  359.7 1.2 fusion.13
  360.9 0.0 all-reduce.4.cloned.1.call-update
  360.9 0.0 all-gather.11.cloned.1.call-start
  361.0 0.0 all-gather.7.cloned.1.call-done
  361.0 3.4 multiply_reduce_fusion.2
  364.4 27.2 %collective-permute-done.2 = bf16[512,1024]{0,1:T(8,128)(2,1)} collective-permute-done((bf16[512,1024]{0,1:T(8,128)(2,1)}, bf16[512,1024]{0,1:T(8,128)(2,1)}, u32[]{:S(2)}, u32[]{:S(2)}) %collective-permute-start.2) | collective-permute-done | bytes 1048608 | tf_op jit(solution)/shard_map/ppermute | solution.py:70
  391.6 1.4 constant_dynamic-update-slice_fusion.7
  393.0 0.0 copy-start.2
  393.0 1.5 constant_dynamic-update-slice_fusion.6
  394.5 1.4 constant_dynamic-update-slice_fusion.5
  395.9 0.1 constant_dynamic-update-slice_fusion.4
  396.1 1.4 constant_dynamic-update-slice_fusion.3
  397.5 1.4 constant_dynamic-update-slice_fusion.2
  398.9 0.0 copy-start.6
  398.9 1.5 constant_dynamic-update-slice_fusion.1
  400.4 0.2 constant_dynamic-update-slice_fusion
  400.6 0.2 copy-done.6
  400.8 4.4 multiply_reduce_fusion
  405.2 14.3 %all-reduce = (f32[]{:T(128)}, f32[]{:T(128)}, f32[]{:T(128)}, f32[]{:T(128)}) all-reduce(f32[]{:T(128)} %multiply_reduce_fusion.1, f32[]{:T(128)} %get-tuple-element.32, f32[]{:T(128)} %multiply_reduce_fusion.3, f32[]{:T(128)} %get-tuple-element.34), channel_id=1, replica_groups=mesh['fs'=4,'rep'=4,'tp'=2] {'fs','tp'}, use_global_device_ids=true, to_apply=%region_1.0 | all-reduce | flops 4 | bytes 32 | tf_op jit(solution)/shard_map/psum | solution.py:79
  420.9 1.2 fusion.11
  422.1 0.0 all-gather.11.cloned.1.call-update
  422.1 0.2 all-gather.9.cloned.1.call-start
  422.3 2.9 copy.27
  426.6 5.4 %fusion.12 = (bf16[512,1024]{0,1:T(8,128)(2,1)}, f32[512,1024]{0,1:T(8,128)}, f32[512,1024]{0,1:T(8,128)}) fusion(f32[512,1024]{0,1:T(8,128)} %copy.27, f32[512,1024]{0,1:T(8,128)} %get-tuple-element.33, f32[]{:T(128)S(6)} %mul.79), kind=kLoop, calls=%fused_computation.31 | loop fusion | flops 1572864 | bytes 9437188 | tf_op jit(solution)/shard_map/convert_element_type | solution.py:95
  432.0 0.0 all-gather.9.cloned.1.call-update
  432.0 0.0 all-reduce.4.cloned.1.call-done
  432.1 1.6 multiply_add_fusion.1
  433.7 1.9 multiply_add_fusion
  435.6 1.0 copy.36
  436.6 2.9 copy.35
  439.5 1.0 copy.30
  440.5 1.0 copy.32
  441.5 2.9 copy.29
  444.4 2.9 copy.31
  447.3 0.2 all-gather.11.cloned.1.call-done
  447.5 2.3 copy.34
  449.7 79.3 %all-gather.9.cloned.1.call-done = bf16[2048,1024]{0,1:T(8,128)(2,1)} async-done(((bf16[512,1024]{0,1:T(8,128)(2,1)}), bf16[2048,1024]{0,1:T(8,128)(2,1)}) %all-gather.9.cloned.1.call-update) | async-done | bytes 4194320 | tf_op jit(solution)/shard_map/all_gather | solution.py:95
  529.1 6.4 %copy.33 = bf16[2048,1024]{1,0:T(8,128)(2,1)} copy(bf16[2048,1024]{0,1:T(8,128)(2,1)} %all-gather.9.cloned.1.call-done) | data formatting | bytes 8388608
  (19 shorter events, 0.1 us)
Async XLA Ops:
  7.2 393.4 %copy-start = (bf16[512,2048]{1,0:T(8,128)(2,1)S(1)}, bf16[512,2048]{1,0:T(8,128)(2,1)}, u32[]{:S(2)}) copy-start(bf16[512,2048]{1,0:T(8,128)(2,1)} %param.20) | copy-start | bytes 6291460
  7.2 233.6 %reduce-scatter.2.cloned.1.call-start = ((), (), s32[]{:S(2)}) async-start(), calls=%async_computation.1 | async-start | bytes 11141120 | tf_op jit(solution)/shard_map/reduce_scatter | solution.py:43
  18.1 267.5 %all-gather.5.cloned.1.call-start = ((), (), s32[]{:S(2)}) async-start(), calls=%async_computation.2 | async-start | bytes 3276800 | tf_op jit(solution)/shard_map/all_gather | solution.py:51
  240.8 46.8 %copy-start.8 = (bf16[16,64,64]{2,1,0:T(8,128)(2,1)S(1)}, bf16[16,64,64]{2,1,0:T(8,128)(2,1)}, u32[]{:S(2)}) copy-start(bf16[16,64,64]{2,1,0:T(8,128)(2,1)} %param.22) | copy-start | bytes 393220
  240.8 120.2 %all-gather.7.cloned.1.call-start = ((), (), s32[]{:S(2)}) async-start(), calls=%async_computation.3 | async-start | bytes 1310720 | tf_op jit(solution)/shard_map/all_gather | solution.py:74
  287.5 28.2 %copy-start.10 = (bf16[4,64,64]{2,1,0:T(8,128)(2,1)S(1)}, bf16[4,64,64]{2,1,0:T(8,128)(2,1)}, u32[]{:S(2)}) copy-start(bf16[4,64,64]{2,1,0:T(8,128)(2,1)} %param.23) | copy-start | bytes 98308
  288.1 1.0 copy-start.1
  289.1 26.6 %collective-permute-start = (bf16[512,1024]{0,1:T(8,128)(2,1)S(1)}, bf16[512,1024]{0,1:T(8,128)(2,1)}, u32[]{:S(2)}, u32[]{:S(2)}) collective-permute-start(bf16[512,1024]{0,1:T(8,128)(2,1)S(1)} %bitcast.30), channel_id=1, source_target_pairs={{0,8},{8,16},{16,24},{24,0},{1,9},{9,17},{17,25},{25,1},{2,10},{10... | collective-permute-start | bytes 3145736 | tf_op jit(solution)/shard_map/ppermute | solution.py:70
  315.7 40.4 %collective-permute-start.1 = (bf16[512,1024]{0,1:T(8,128)(2,1)}, bf16[512,1024]{0,1:T(8,128)(2,1)}, u32[]{:S(2)}, u32[]{:S(2)}) collective-permute-start(bf16[512,1024]{0,1:T(8,128)(2,1)} %collective-permute-done), channel_id=1, source_target_pairs={{0,8},{8,16},{16,24},{24,0},{1,9},{9,17},{17,25},{25,1},{2,10},{10... | collective-permute-start | bytes 3145736 | tf_op jit(solution)/shard_map/ppermute | solution.py:70
  316.7 115.3 %all-reduce.4.cloned.1.call-start = ((), (), s32[]{:S(2)}) async-start(), calls=%async_computation.6 | async-start | bytes 1310720 | tf_op jit(solution)/shard_map/psum | solution.py:55
  356.1 35.5 %collective-permute-start.2 = (bf16[512,1024]{0,1:T(8,128)(2,1)}, bf16[512,1024]{0,1:T(8,128)(2,1)}, u32[]{:S(2)}, u32[]{:S(2)}) collective-permute-start(bf16[512,1024]{0,1:T(8,128)(2,1)} %collective-permute-done.1), channel_id=1, source_target_pairs={{0,8},{8,16},{16,24},{24,0},{1,9},{9,17},{17,25},{25,1},{2,10},{10... | collective-permute-start | bytes 3145736 | tf_op jit(solution)/shard_map/ppermute | solution.py:70
  360.9 86.6 %all-gather.11.cloned.1.call-start = ((), (), s32[]{:S(2)}) async-start(), calls=%async_computation.5 | async-start | bytes 1310720 | tf_op jit(solution)/shard_map/all_gather | solution.py:96
  393.0 2.9 copy-start.2
  398.9 1.9 copy-start.6
  400.8 20.1 %copy-start.3 = (f32[512,256]{0,1:T(8,128)S(1)}, f32[512,256]{0,1:T(8,128)}, u32[]{:S(2)}) copy-start(f32[512,256]{0,1:T(8,128)} %copy.28) | copy-start | bytes 1572868
  422.1 107.0 %all-gather.9.cloned.1.call-start = ((), (), s32[]{:S(2)}) async-start(), calls=%async_computation.4 | async-start | bytes 5242880 | tf_op jit(solution)/shard_map/all_gather | solution.py:95
  426.5 5.5 %copy-start.9 = (f32[4,64,64]{2,1,0:T(8,128)S(1)}, f32[4,64,64]{2,1,0:T(8,128)}, u32[]{:S(2)}) copy-start(f32[4,64,64]{2,1,0:T(8,128)} %param.25) | copy-start | bytes 196612
  426.6 7.1 %copy-start.7 = (f32[16,64,64]{2,1,0:T(8,128)S(1)}, f32[16,64,64]{2,1,0:T(8,128)}, u32[]{:S(2)}) copy-start(f32[16,64,64]{2,1,0:T(8,128)} %param.24) | copy-start | bytes 786436
  435.6 3.9 copy-start.5
  436.6 3.9 copy-start.4
Sparse Core Ops, SparseCore 0:
  18.2 222.5 reduce-scatter.1
  242.6 42.9 all-gather.4
  316.8 42.4 all-gather.6
  362.8 47.3 all-reduce.3
  422.2 25.2 all-gather.10
  448.9 80.1 all-gather.8
